TPU v7x, 32 devices: a whole 2x2x4 slice. The times are simulated.
32 devices in a mesh: ep: 4 (over y, x), tp: 8 (over z, core).
Axes of the slice: x: 2, y: 2, z: 4, core: 2. Of those that a mesh axis runs over, the one named last changes fastest.
Arguments:
- pool_input: bfloat16 [4096, 1024], P('ep', 'tp'), may hold values from -6 to 6
- pool_gain: float32 [1024], P('tp'), may hold values from 0.1 to 1.9
- mix_weight: bfloat16 [1024, 2048], P('tp'), may hold values from -0.1875 to 0.1875
- moe_input: bfloat16 [8192, 2048], P(('ep', 'tp')), may hold values from -6 to 6
- moe_gain: float32 [2048], replicated, may hold values from 0.1 to 1.9
- expert_ids: int32 [8192, 2], P(('ep', 'tp')), may hold values from 0 to 15, as said below
- route_weight: float32 [8192, 2], P(('ep', 'tp')), may hold values from 0.2 to 1
- gate_weight: bfloat16 [16, 2048, 1024], P('ep', None, 'tp'), may hold values from -0.125 to 0.125
- up_weight: bfloat16 [16, 2048, 1024], P('ep', None, 'tp'), may hold values from -0.125 to 0.125
- down_weight: bfloat16 [16, 2048, 1024], P('ep', None, 'tp'), may hold values from -0.1875 to 0.1875
Outputs:
- mixed_out: bfloat16 [4096, 2048], P(('ep', 'tp'))
- moe_out: bfloat16 [8192, 2048], P(('ep', 'tp'))
Inputs may be any that keep to these rules, and one draw needn't show every extreme that they name: `expert_ids`: each row names 2 different experts of one group of 4 consecutive experts. In each aligned block of 256 rows (the rows of one device) no expert is named by more than 48 rows, and some expert is named by exactly 48 rows.
All inputs are finite; a program needn't handle non-finite values.
Results may differ from a plain program's by a relative error of at most 0.012.
Values may be sent and summed in bfloat16 or wider, within the bound.
A program may use at most 128 MiB of HBM per device.

v0:
```python
import jax
import jax.numpy as jnp
from jax import lax
from jax.sharding import PartitionSpec as P

GROUP_CH = 256
EXPERTS = 16
TOP = 2
CAP = 48
eps_norm = 1e-06


def from_behind(shard, axis, by):
    peers = lax.axis_size(axis)
    pairs = [(i, i + by) for i in range(peers) if 0 <= i + by < peers]
    return lax.ppermute(shard, axis, pairs)


def window_sums(extended, row_count):
    level_sum = extended
    stride = 1
    outputs = []
    for doubling in range(4):
        level_sum = level_sum[stride:] + level_sum[:-stride]
        stride = stride * 2
        outputs.append(level_sum[level_sum.shape[0] - row_count :])
    return outputs


def pool_mixer(pool_input, pool_gain):
    row_count, channels = pool_input.shape
    carried = from_behind(pool_input[row_count - 15 :], "ep", 1)
    extended = jnp.concatenate([carried, pool_input], axis=0).astype(jnp.float32)
    window_list = window_sums(extended, row_count)
    channel_ids = lax.axis_index("tp") * channels + lax.iota(jnp.int32, channels)
    group_ids = channel_ids // GROUP_CH
    position = lax.axis_index("ep") * row_count + lax.iota(jnp.int32, row_count)
    summed = jnp.zeros((row_count, channels), jnp.float32)
    widths = jnp.zeros((channels,), jnp.int32)
    for index_group in range(4):
        inside = group_ids == index_group
        summed = jnp.where(inside[None, :], window_list[index_group], summed)
        widths = jnp.where(inside, 2 ** (index_group + 1), widths)
    counted = jnp.minimum(position[:, None] + 1, widths[None, :]).astype(jnp.float32)
    values = extended[15:]
    return ((summed / counted - values) * pool_gain).astype(jnp.bfloat16)


def route_slots(expert_ids):
    flat_ids = expert_ids.reshape(-1)
    marked = (flat_ids[:, None] == lax.iota(jnp.int32, EXPERTS)[None, :]).astype(jnp.int32)
    before_count = jnp.cumsum(marked, axis=0) - marked
    ranked = jnp.sum(before_count * marked, axis=1)
    return (flat_ids * CAP + ranked).reshape(expert_ids.shape)


def body(
    pool_input,
    pool_gain,
    mix_weight,
    moe_input,
    moe_gain,
    expert_ids,
    route_weight,
    gate_weight,
    up_weight,
    down_weight,
):
    pooled = pool_mixer(pool_input, pool_gain)
    regrouped = lax.all_to_all(pooled, "tp", split_axis=0, concat_axis=1, tiled=True)
    mixed_sum = jnp.dot(
        regrouped,
        lax.all_gather(mix_weight, "tp", axis=0, tiled=True),
        preferred_element_type=jnp.float32,
    )
    mixed_out = mixed_sum.astype(jnp.bfloat16)
    inputs = moe_input.astype(jnp.float32)
    scale_rows = lax.rsqrt(jnp.mean(inputs * inputs, axis=-1, keepdims=True) + eps_norm)
    normed = (inputs * scale_rows * moe_gain).astype(jnp.bfloat16)
    slots = route_slots(expert_ids)
    slot_index = lax.iota(jnp.int32, EXPERTS * CAP)
    placing = (
        (slot_index[:, None] == slots[None, :, 0]) | (slot_index[:, None] == slots[None, :, 1])
    ).astype(jnp.bfloat16)
    outgoing = jnp.dot(placing, normed, preferred_element_type=jnp.float32).astype(jnp.bfloat16)
    outgoing = outgoing.reshape(EXPERTS, CAP, normed.shape[1])
    arrived = lax.all_to_all(outgoing, "ep", split_axis=0, concat_axis=1, tiled=True)
    gate_piece = lax.all_gather(gate_weight, "tp", axis=2, tiled=True)
    up_piece = lax.all_gather(up_weight, "tp", axis=2, tiled=True)
    down_piece = lax.all_gather(down_weight, "tp", axis=2, tiled=True)
    gate_part = jnp.einsum("erd,edf->erf", arrived, gate_piece, preferred_element_type=jnp.float32)
    upward = jnp.einsum("erd,edf->erf", arrived, up_piece, preferred_element_type=jnp.float32)
    hidden = (jax.nn.silu(gate_part) * upward).astype(jnp.bfloat16)
    expert_sum = jnp.einsum("erf,edf->erd", hidden, down_piece, preferred_element_type=jnp.float32)
    expert_rows = expert_sum.astype(jnp.bfloat16)
    returned = lax.all_to_all(expert_rows, "ep", split_axis=1, concat_axis=0, tiled=True)
    returned_rows = returned.reshape(EXPERTS * CAP, returned.shape[2])
    combined = jnp.zeros((normed.shape[0], normed.shape[1]), jnp.float32)
    for route_index in range(TOP):
        picking = (slots[:, route_index][:, None] == slot_index[None, :]).astype(jnp.bfloat16)
        chosen_rows = jnp.dot(picking, returned_rows, preferred_element_type=jnp.float32)
        combined = combined + route_weight[:, route_index : route_index + 1] * chosen_rows
    moe_out = combined.astype(jnp.bfloat16)
    return (mixed_out, moe_out)


def solution(mesh):
    return jax.shard_map(
        body,
        mesh=mesh,
        in_specs=(
            P("ep", "tp"),
            P("tp"),
            P("tp", None),
            P(("ep", "tp"), None),
            P(),
            P(("ep", "tp"), None),
            P(("ep", "tp"), None),
            P("ep", None, "tp"),
            P("ep", None, "tp"),
            P("ep", None, "tp"),
        ),
        out_specs=(P(("ep", "tp"), None), P(("ep", "tp"), None)),
        check_vma=False,
    )
```

profile of v0, /device:TPU:0, one launch (start us, length us, event | category | flops | bytes accessed | tf_op | source)
XLA Modules:
  0.0 554.3 jit_solution(15557223583954882724)
XLA Ops:
  7.2 0.0 copy-start.5
  7.2 0.0 copy-start.1
  7.2 0.0 all-gather.7.cloned.1.call-start
  7.2 0.7 all-gather.7.cloned.1.call-update
  7.9 0.0 copy-start.4
  7.9 0.0 all-gather.11.cloned.1.call-start
  8.0 0.7 all-gather.11.cloned.1.call-update
  8.7 0.0 all-gather.9.cloned.1.call-start
  8.7 0.7 all-gather.9.cloned.1.call-update
  9.4 0.0 copy-done.5
  9.4 0.1 copy.47
  9.6 0.1 eq.138
  9.7 0.1 eq.134
  9.9 1.2 reduce-window.6
  11.0 0.2 slice_reduce_fusion
  11.3 0.1 fusion.23
  11.4 0.1 reduce_sum.21
  11.5 0.1 copy.50
  11.6 0.0 copy-done.1
  11.6 0.3 fusion.2
  11.9 0.0 copy-done.4
  12.0 2.8 convolution_convert_fusion
  14.7 0.0 copy-start.3
  14.7 5.3 all-to-all-start.1
  20.0 0.0 copy-start.7
  20.0 0.0 all-gather.5.cloned.1.call-start
  20.1 0.0 copy-done.3
  20.1 3.9 collective-permute-start
  24.0 0.0 all-gather.5.cloned.1.call-update
  24.1 30.0 %collective-permute-done = bf16[15,128]{1,0:T(8,128)(2,1)S(1)} collective-permute-done((bf16[15,128]{1,0:T(8,128)(2,1)S(1)}, bf16[15,128]{1,0:T(8,128)(2,1)S(1)}, u32[]{:S(2)}, u32[]{:S(2)}) %collective-permute-start) | collective-permute-done | bytes 3872 | tf_op jit(solution)/shard_map/ppermute | solution.py:16
  54.1 0.1 maximum_convert_fusion
  54.2 0.1 slice_add_fusion.1
  54.2 0.1 slice_add_fusion
  54.3 0.1 slice_add_fusion.2
  54.3 0.0 copy-done.7
  54.4 1.1 fusion.12
  55.4 0.8 all-to-all-done.1
  56.2 5.2 all-to-all-start
  61.4 1.9 copy.51
  63.3 107.9 %all-gather.7.cloned.1.call-done = bf16[4,2048,1024]{2,1,0:T(8,128)(2,1)} async-done(((bf16[4,2048,128]{2,1,0:T(8,128)(2,1)}), bf16[4,2048,1024]{2,1,0:T(8,128)(2,1)}) %all-gather.7.cloned.1.call-update) | async-done | bytes 16777232 | tf_op jit(solution)/shard_map/all_gather | solution.py:88
  171.2 0.0 copy-start
  171.2 11.9 %fusion.28 = f32[4,192,1024]{2,1,0:T(8,128)} fusion(bf16[4,192,2048]{2,1,0:T(8,128)(2,1)} %bitcast.48, bf16[4,2048,1024]{2,1,0:T(8,128)(2,1)} %all-gather.7.cloned.1.call-done), kind=kOutput, calls=%fused_computation.62 | convolution fusion | flops 3221225472 | bytes 23068672 | tf_op jit(solution)/shard_map/erd,edf->erf/dot_general | solution.py:91
  183.2 142.6 %all-gather.11.cloned.1.call-done = bf16[4,2048,1024]{2,1,0:T(8,128)(2,1)} async-done(((bf16[4,2048,128]{2,1,0:T(8,128)(2,1)}), bf16[4,2048,1024]{2,1,0:T(8,128)(2,1)}) %all-gather.11.cloned.1.call-update) | async-done | bytes 16777232 | tf_op jit(solution)/shard_map/all_gather | solution.py:90
  325.8 151.6 %all-gather.9.cloned.1.call-done = bf16[4,2048,1024]{2,1,0:T(8,128)(2,1)} async-done(((bf16[4,2048,128]{2,1,0:T(8,128)(2,1)}), bf16[4,2048,1024]{2,1,0:T(8,128)(2,1)}) %all-gather.9.cloned.1.call-update) | async-done | bytes 16777232 | tf_op jit(solution)/shard_map/all_gather | solution.py:89
  477.4 0.0 copy-done
  477.4 17.7 %convolution_convert_fusion.1 = bf16[4,192,2048]{2,1,0:T(8,128)(2,1)} fusion(bf16[4,2048,1024]{2,1,0:T(8,128)(2,1)} %all-gather.11.cloned.1.call-done, f32[4,192,1024]{2,1,0:T(8,128)} %fusion.28, bf16[4,192,2048]{2,1,0:T(8,128)(2,1)S(1)} %bitcast.49, bf16[4,2048,1024]{2,1,0:T(8,128)(2,1)} %all-gather.9.cloned.1.call-done), kind=kOutput, calls=%fused_computation.1 | convolution fusion | flops 6448742400 | bytes 42991616 | tf_op jit(solution)/shard_map/erf,edf->erd/dot_general | solution.py:94
  495.1 6.0 %copy.52 = bf16[4,192,2048]{2,0,1:T(4,128)(2,1)} copy(bf16[4,192,2048]{2,1,0:T(8,128)(2,1)} %convolution_convert_fusion.1) | data formatting | bytes 6291456 | tf_op jit(solution)/shard_map/convert_element_type | solution.py:95
  501.1 0.0 copy-start.6
  501.1 0.0 all-to-all-done
  501.1 0.0 copy-start.2
  501.1 0.7 copy-done.2
  501.8 3.9 all-to-all-start.2
  505.7 0.0 copy-done.6
  505.7 1.1 copy.46
  506.9 17.0 %all-gather.5.cloned.1.call-done = bf16[1024,2048]{1,0:T(8,128)(2,1)} async-done(((bf16[128,2048]{1,0:T(8,128)(2,1)}), bf16[1024,2048]{1,0:T(8,128)(2,1)}) %all-gather.5.cloned.1.call-update) | async-done | bytes 4194320 | tf_op jit(solution)/shard_map/all_gather | solution.py:73
  523.9 3.7 convolution_convert_fusion.2
  527.6 14.8 %all-to-all-done.2 = bf16[4,192,2048]{2,0,1:T(4,128)(2,1)S(1)} async-done(((bf16[4,192,2048]{2,0,1:T(4,128)(2,1)}), bf16[4,192,2048]{2,0,1:T(4,128)(2,1)S(1)}, u32[]{:S(2)}, u32[]{:S(2)}) %all-to-all-start.2) | async-done | bytes 3145760 | tf_op jit(solution)/shard_map/all_to_all | solution.py:96
  542.5 1.7 copy.53
  544.2 0.4 copy.54
  544.6 1.0 convolution_multiply_fusion.1
  545.7 2.1 fusion.1
  (12 shorter events, 0.1 us)
Async XLA Ops:
  7.2 2.3 copy-start.5
  7.2 4.4 copy-start.1
  7.2 164.1 %all-gather.7.cloned.1.call-start = ((), (), s32[]{:S(2)}) async-start(), calls=%async_computation.4 | async-start | bytes 18874368 | tf_op jit(solution)/shard_map/all_gather | solution.py:88
  7.9 4.0 copy-start.4
  7.9 317.8 %all-gather.11.cloned.1.call-start = ((), (), s32[]{:S(2)}) async-start(), calls=%async_computation.6 | async-start | bytes 18874368 | tf_op jit(solution)/shard_map/all_gather | solution.py:90
  8.7 468.7 %all-gather.9.cloned.1.call-start = ((), (), s32[]{:S(2)}) async-start(), calls=%async_computation.5 | async-start | bytes 18874368 | tf_op jit(solution)/shard_map/all_gather | solution.py:89
  14.7 5.3 copy-start.3
  14.7 41.5 %all-to-all-start.1 = ((bf16[16,48,2048]{2,1,0:T(8,128)(2,1)}), bf16[16,48,2048]{2,1,0:T(8,128)(2,1)S(1)}, u32[]{:S(2)}, u32[]{:S(2)}) async-start(bf16[16,48,2048]{2,1,0:T(8,128)(2,1)} %bitcast.7), calls=%async_computation.1 | async-start | bytes 6291456 | tf_op jit(solution)/shard_map/all_to_all | solution.py:87
  20.0 34.3 %copy-start.7 = (f32[128]{0:T(128)S(1)}, f32[128]{0:T(128)}, u32[]{:S(2)}) copy-start(f32[128]{0:T(128)} %param.11) | copy-start | bytes 1540
  20.0 503.9 %all-gather.5.cloned.1.call-start = ((), (), s32[]{:S(2)}) async-start(), calls=%async_computation.3 | async-start | bytes 4718592 | tf_op jit(solution)/shard_map/all_gather | solution.py:73
  20.1 34.0 %collective-permute-start = (bf16[15,128]{1,0:T(8,128)(2,1)S(1)}, bf16[15,128]{1,0:T(8,128)(2,1)S(1)}, u32[]{:S(2)}, u32[]{:S(2)}) collective-permute-start(bf16[15,128]{1,0:T(8,128)(2,1)S(1)} %slice.57), channel_id=1, source_target_pairs={{0,8},{8,16},{16,24},{1,9},{9,17},{17,25},{2,10},{10,18},{18,26},{... | collective-permute-start | bytes 11528 | tf_op jit(solution)/shard_map/ppermute | solution.py:16
  56.2 444.9 %all-to-all-start = ((bf16[8,128,128]{2,1,0:T(8,128)(2,1)}), bf16[8,128,128]{2,1,0:T(8,128)(2,1)S(1)}, u32[]{:S(2)}, u32[]{:S(2)}) async-start(bf16[8,128,128]{2,1,0:T(8,128)(2,1)} %bitcast), calls=%async_computation | async-start | bytes 524288 | tf_op jit(solution)/shard_map/all_to_all | solution.py:70
  171.2 306.1 %copy-start = (bf16[4,4,48,2048]{3,2,0,1:T(8,128)(2,1)S(1)}, bf16[4,4,48,2048]{3,2,0,1:T(8,128)(2,1)}, u32[]{:S(2)}) copy-start(bf16[4,4,48,2048]{3,2,0,1:T(8,128)(2,1)} %copy.51) | copy-start | bytes 9437188
  501.1 4.6 copy-start.6
  501.1 0.7 copy-start.2
  501.8 40.6 %all-to-all-start.2 = ((bf16[4,192,2048]{2,0,1:T(4,128)(2,1)}), bf16[4,192,2048]{2,0,1:T(4,128)(2,1)S(1)}, u32[]{:S(2)}, u32[]{:S(2)}) async-start(bf16[4,192,2048]{2,0,1:T(4,128)(2,1)} %copy.52), calls=%async_computation.2 | async-start | bytes 6291456 | tf_op jit(solution)/shard_map/all_to_all | solution.py:96
Sparse Core Ops, SparseCore 0:
  9.6 161.6 all-gather.6
  172.8 152.8 all-gather.10
  327.4 149.9 all-gather.8
  478.8 45.0 all-gather.4
where the time goes:
time: 555 us; the launch traced here: 554 us
  waiting for transfers between devices  467 us (84%)
  matrix products  39.2 us (7%)
  starting transfers between devices  18.4 us (3%)
  between operations  14 us (3%)
  local copies, waits for them, and re-layouts  12.8 us (2%)
    all_gather x1, waiting for transfers between devices, body(): up_piece = lax.all_gather(up_weight, 'tp', axis=2, tiled=True)  152 us
    all_gather x1, waiting for transfers between devices, body(): down_piece = lax.all_gather(down_weight, 'tp', axis=2, tiled=True)  143 us
    all_gather x1, waiting for transfers between devices, body(): gate_piece = lax.all_gather(gate_weight, 'tp', axis=2, tiled=True)  108 us
    ppermute x1, waiting for transfers between devices, from_behind(): return lax.ppermute(shard, axis, pairs)  30 us
    dot_general x1, matrix products, body(): jnp.einsum('erf,edf->erd', hidden, down_piece, preferred_element_type=jnp...  17.7 us
    all_gather x1, waiting for transfers between devices, body(): lax.all_gather(mix_weight, 'tp', axis=0, tiled=True)  17 us
    all_to_all x1, waiting for transfers between devices, body(): lax.all_to_all(expert_rows, 'ep', split_axis=1, concat_axis=0, tiled=True)  14.8 us
    dot_general x1, matrix products, body(): jnp.einsum('erd,edf->erf', arrived, gate_piece, preferred_element_type=jn...  11.9 us
  transfers between devices with their start and end apart: 8, of which 7 were waited for; matrix products, arithmetic and copies ran while one was open for 9% of the time, Pallas kernels for 0%

commit v1 on v0

--- a/solution.py
+++ b/solution.py
@@ -8,6 +8,21 @@
 TOP = 2
 CAP = 48
 eps_norm = 1e-06
+
+
+def on_each_block(array, axis, dim, make, out_dim):
+    ways, here, step = (lax.axis_size(axis), lax.axis_index(axis), array.shape[dim])
+    results = []
+    for far in range(ways):
+        arriving = (
+            lax.ppermute(array, axis, [(d, (d + 1) % ways) for d in range(ways)])
+            if far + 1 < ways
+            else array
+        )
+        results.append(make(array, (here - far) % ways * step))
+        array = arriving
+    line = jnp.concatenate(results[::-1], axis=out_dim)
+    return jnp.roll(line, (here + 1) * results[0].shape[out_dim], axis=out_dim)
 
 
 def from_behind(shard, axis, by):
@@ -85,10 +100,17 @@
     outgoing = jnp.dot(placing, normed, preferred_element_type=jnp.float32).astype(jnp.bfloat16)
     outgoing = outgoing.reshape(EXPERTS, CAP, normed.shape[1])
     arrived = lax.all_to_all(outgoing, "ep", split_axis=0, concat_axis=1, tiled=True)
-    gate_piece = lax.all_gather(gate_weight, "tp", axis=2, tiled=True)
     up_piece = lax.all_gather(up_weight, "tp", axis=2, tiled=True)
     down_piece = lax.all_gather(down_weight, "tp", axis=2, tiled=True)
-    gate_part = jnp.einsum("erd,edf->erf", arrived, gate_piece, preferred_element_type=jnp.float32)
+    gate_part = on_each_block(
+        gate_weight,
+        "tp",
+        2,
+        lambda shard_2, start: jnp.einsum(
+            "erd,edf->erf", arrived, shard_2, preferred_element_type=jnp.float32
+        ),
+        2,
+    )
     upward = jnp.einsum("erd,edf->erf", arrived, up_piece, preferred_element_type=jnp.float32)
     hidden = (jax.nn.silu(gate_part) * upward).astype(jnp.bfloat16)
     expert_sum = jnp.einsum("erf,edf->erd", hidden, down_piece, preferred_element_type=jnp.float32)

time: 555 us -> 582 us (1.049)
  the two profiles are of different devices: /device:TPU:0 before, /device:TPU:16 now
where the time goes in v1:
time: 582 us; the launch traced here: 581 us
  waiting for transfers between devices  450 us (77%)
  matrix products  46.2 us (8%)
  starting transfers between devices  42.8 us (7%)
  local copies, waits for them, and re-layouts  24.9 us (4%)
  between operations  14 us (2%)
    ppermute x7, waiting for transfers between devices, on_each_block(): lax.ppermute(array, axis, [(d, (d + 1) % ways) for d in range(ways)])  433 us
    ppermute x7, starting transfers between devices, on_each_block(): lax.ppermute(array, axis, [(d, (d + 1) % ways) for d in range(ways)])  26.7 us
    dot_general x8, matrix products, body(): jnp.einsum('erd,edf->erf', arrived, shard_2, preferred_element_type=jnp.f...  19.2 us
    dot_general x1, matrix products, body(): jnp.einsum('erf,edf->erd', hidden, down_piece, preferred_element_type=jnp...  17.3 us
    all_to_all x1, waiting for transfers between devices, body(): lax.all_to_all(expert_rows, 'ep', split_axis=1, concat_axis=0, tiled=True)  15.8 us
    unnamed x44, local copies, waits for them, and re-layouts  12.1 us
  transfers between devices with their start and end apart: 14, of which 8 were waited for; matrix products, arithmetic and copies ran while one was open for 11% of the time, Pallas kernels for 0%

profile of v1, /device:TPU:16, one launch (start us, length us, event | category | flops | bytes accessed | tf_op | source)
XLA Modules:
  0.0 581.0 jit_solution(3101445564384831360)
XLA Ops:
  7.3 0.7 all-gather.6.cloned.1.call-update
  8.0 0.7 all-gather.8.cloned.1.call-update
  8.7 0.1 copy-done.1
  8.8 70.4 %collective-permute-done.1 = bf16[4,2048,128]{2,1,0:T(8,128)(2,1)S(1)} collective-permute-done((bf16[4,2048,128]{2,1,0:T(8,128)(2,1)S(1)}, bf16[4,2048,128]{2,1,0:T(8,128)(2,1)S(1)}, u32[]{:S(2)}, u32[]{:S(2)}) %collective-permute-start.1) | collective-permute-done | bytes 2097184 | tf_op jit(solution)/shard_map/ppermute | solution.py:18
  79.2 1.3 copy-done.3
  80.5 1.5 collective-permute-start.2
  82.0 68.9 %collective-permute-done.2 = bf16[4,2048,128]{2,1,0:T(8,128)(2,1)S(1)} collective-permute-done((bf16[4,2048,128]{2,1,0:T(8,128)(2,1)S(1)}, bf16[4,2048,128]{2,1,0:T(8,128)(2,1)S(1)}, u32[]{:S(2)}, u32[]{:S(2)}) %collective-permute-start.2) | collective-permute-done | bytes 2097184 | tf_op jit(solution)/shard_map/ppermute | solution.py:18
  150.9 1.4 copy-done.5
  152.3 18.6 %collective-permute-start.3 = (bf16[4,2048,128]{2,1,0:T(8,128)(2,1)S(1)}, bf16[4,2048,128]{2,1,0:T(8,128)(2,1)S(1)}, u32[]{:S(2)}, u32[]{:S(2)}) collective-permute-start(bf16[4,2048,128]{2,1,0:T(8,128)(2,1)S(1)} %collective-permute-done.2), channel_id=1, source_target_pairs={{0,1},{1,2},{2,3},{3,4},{4,5},{5,6},{6,7},{7,0},{8,9},{9,10},{10,1... | collective-permute-start | bytes 6291464 | tf_op jit(solution)/shard_map/ppermute | solution.py:18
  170.9 49.2 %collective-permute-done.3 = bf16[4,2048,128]{2,1,0:T(8,128)(2,1)S(1)} collective-permute-done((bf16[4,2048,128]{2,1,0:T(8,128)(2,1)S(1)}, bf16[4,2048,128]{2,1,0:T(8,128)(2,1)S(1)}, u32[]{:S(2)}, u32[]{:S(2)}) %collective-permute-start.3) | collective-permute-done | bytes 2097184 | tf_op jit(solution)/shard_map/ppermute | solution.py:18
  220.0 1.4 copy-done.7
  221.4 70.4 %collective-permute-done.4 = bf16[4,2048,128]{2,1,0:T(8,128)(2,1)S(1)} collective-permute-done((bf16[4,2048,128]{2,1,0:T(8,128)(2,1)S(1)}, bf16[4,2048,128]{2,1,0:T(8,128)(2,1)S(1)}, u32[]{:S(2)}, u32[]{:S(2)}) %collective-permute-start.4) | collective-permute-done | bytes 2097184 | tf_op jit(solution)/shard_map/ppermute | solution.py:18
  291.8 1.3 copy-done.9
  293.1 71.4 %collective-permute-done.5 = bf16[4,2048,128]{2,1,0:T(8,128)(2,1)} collective-permute-done((bf16[4,2048,128]{2,1,0:T(8,128)(2,1)S(1)}, bf16[4,2048,128]{2,1,0:T(8,128)(2,1)}, u32[]{:S(2)}, u32[]{:S(2)}) %collective-permute-start.5) | collective-permute-done | bytes 2097184 | tf_op jit(solution)/shard_map/ppermute | solution.py:18
  364.5 6.6 %collective-permute-start.6 = (bf16[4,2048,128]{2,1,0:T(8,128)(2,1)}, bf16[4,2048,128]{2,1,0:T(8,128)(2,1)}, u32[]{:S(2)}, u32[]{:S(2)}) collective-permute-start(bf16[4,2048,128]{2,1,0:T(8,128)(2,1)} %collective-permute-done.5), channel_id=1, source_target_pairs={{0,1},{1,2},{2,3},{3,4},{4,5},{5,6},{6,7},{7,0},{8,9},{9,10},{10,1... | collective-permute-start | bytes 6291464 | tf_op jit(solution)/shard_map/ppermute | solution.py:18
  371.1 0.1 copy.47
  371.3 0.1 eq.141
  371.4 0.1 eq.137
  371.6 1.2 reduce-window.6
  372.7 0.2 slice_reduce_fusion
  373.0 0.1 fusion.23
  373.1 0.1 reduce_sum.21
  373.2 0.1 copy.50
  373.3 0.3 fusion.2
  373.7 2.8 convolution_convert_fusion
  376.5 3.8 all-to-all-start.1
  380.3 0.0 all-gather.4.cloned.1.call-start
  380.4 3.8 collective-permute-start
  384.3 46.8 %collective-permute-done.6 = bf16[4,2048,128]{2,1,0:T(8,128)(2,1)} collective-permute-done((bf16[4,2048,128]{2,1,0:T(8,128)(2,1)}, bf16[4,2048,128]{2,1,0:T(8,128)(2,1)}, u32[]{:S(2)}, u32[]{:S(2)}) %collective-permute-start.6) | collective-permute-done | bytes 2097184 | tf_op jit(solution)/shard_map/ppermute | solution.py:18
  431.1 0.1 maximum_convert_fusion
  431.2 0.1 slice_add_fusion.1
  431.3 0.1 slice_add_fusion
  431.3 0.1 slice_add_fusion.2
  431.4 1.1 fusion.12
  432.5 4.5 all-to-all-start
  437.0 2.1 copy.51
  439.1 55.7 %collective-permute-done.7 = bf16[4,2048,128]{2,1,0:T(8,128)(2,1)} collective-permute-done((bf16[4,2048,128]{2,1,0:T(8,128)(2,1)}, bf16[4,2048,128]{2,1,0:T(8,128)(2,1)}, u32[]{:S(2)}, u32[]{:S(2)}) %collective-permute-start.7) | collective-permute-done | bytes 2097184 | tf_op jit(solution)/shard_map/ppermute | solution.py:18
  494.8 3.3 constant_dynamic-update-slice_fusion.15
  498.1 3.3 constant_dynamic-update-slice_fusion.14
  501.5 3.5 constant_dynamic-update-slice_fusion.13
  505.0 1.8 constant_dynamic-update-slice_fusion.12
  506.8 1.8 constant_dynamic-update-slice_fusion.11
  508.6 1.8 constant_dynamic-update-slice_fusion.10
  510.4 1.9 constant_dynamic-update-slice_fusion.9
  512.3 1.8 constant_dynamic-update-slice_fusion.8
  514.1 0.8 constant_dynamic-update-slice_fusion.7
  514.9 0.9 constant_dynamic-update-slice_fusion.6
  515.8 0.8 constant_dynamic-update-slice_fusion.5
  516.6 0.8 constant_dynamic-update-slice_fusion.4
  517.4 0.8 constant_dynamic-update-slice_fusion.3
  518.3 0.8 constant_dynamic-update-slice_fusion.2
  519.1 0.8 constant_dynamic-update-slice_fusion.1
  519.8 0.8 constant_dynamic-update-slice_fusion
  520.6 17.3 %convolution_convert_fusion.1 = bf16[4,192,2048]{2,1,0:T(8,128)(2,1)} fusion(bf16[4,2048,1024]{2,1,0:T(8,128)(2,1)} %all-gather.8.cloned.1.call-done, f32[4,192,2048]{2,1,0:T(8,128)} %constant_dynamic-update-slice_fusion, s32[]{:T(128)S(6)} %select_n.86, bf16[4,192,2048]{2,1,0:T(8,128)(2,1)S(1)} %bitcast.66, ...), kind=kOutput, calls=%fused_computation.1 | convolution fusion | flops 6448742400 | bytes 42991620 | tf_op jit(solution)/shard_map/erf,edf->erd/dot_general | solution.py:116
  538.0 5.9 %copy.52 = bf16[4,192,2048]{2,0,1:T(4,128)(2,1)} copy(bf16[4,192,2048]{2,1,0:T(8,128)(2,1)} %convolution_convert_fusion.1) | data formatting | bytes 6291456 | tf_op jit(solution)/shard_map/convert_element_type | solution.py:117
  543.9 0.7 copy-done.12
  544.6 3.9 all-to-all-start.2
  548.5 1.1 copy.46
  549.7 3.7 convolution_convert_fusion.2
  553.4 15.8 %all-to-all-done.2 = bf16[4,192,2048]{2,0,1:T(4,128)(2,1)S(1)} async-done(((bf16[4,192,2048]{2,0,1:T(4,128)(2,1)}), bf16[4,192,2048]{2,0,1:T(4,128)(2,1)S(1)}, u32[]{:S(2)}, u32[]{:S(2)}) %all-to-all-start.2) | async-done | bytes 3145760 | tf_op jit(solution)/shard_map/all_to_all | solution.py:118
  569.2 1.7 copy.53
  570.9 0.4 copy.54
  571.3 1.0 convolution_multiply_fusion.1
  572.4 2.1 fusion.1
  (55 shorter events, 0.3 us)
Async XLA Ops:
  7.2 1.6 copy-start.1
  7.2 364.0 %copy-start.15 = (s32[256,2]{0,1:T(2,128)S(1)}, s32[256,2]{0,1:T(2,128)}, u32[]{:S(2)}) copy-start(s32[256,2]{0,1:T(2,128)} %param.15) | copy-start | bytes 6148
  7.2 366.1 %copy-start.11 = (bf16[256,2048]{1,0:T(8,128)(2,1)S(1)}, bf16[256,2048]{1,0:T(8,128)(2,1)}, u32[]{:S(2)}) copy-start(bf16[256,2048]{1,0:T(8,128)(2,1)} %param.13) | copy-start | bytes 3145732
  7.2 366.5 %copy-start.14 = (f32[2048]{0:T(1024)S(1)}, f32[2048]{0:T(1024)}, u32[]{:S(2)}) copy-start(f32[2048]{0:T(1024)} %param.14) | copy-start | bytes 24580
  7.2 513.4 %all-gather.6.cloned.1.call-start = ((), (), s32[]{:S(2)}) async-start(), calls=%async_computation.4 | async-start | bytes 18874368 | tf_op jit(solution)/shard_map/all_gather | solution.py:103
  7.9 512.7 %all-gather.8.cloned.1.call-start = ((), (), s32[]{:S(2)}) async-start(), calls=%async_computation.5 | async-start | bytes 18874368 | tf_op jit(solution)/shard_map/all_gather | solution.py:104
  8.8 70.4 %collective-permute-start.1 = (bf16[4,2048,128]{2,1,0:T(8,128)(2,1)S(1)}, bf16[4,2048,128]{2,1,0:T(8,128)(2,1)S(1)}, u32[]{:S(2)}, u32[]{:S(2)}) collective-permute-start(bf16[4,2048,128]{2,1,0:T(8,128)(2,1)S(1)} %copy-done.1), channel_id=1, source_target_pairs={{0,1},{1,2},{2,3},{3,4},{4,5},{5,6},{6,7},{7,0},{8,9},{9,10},{10,1... | collective-permute-start | bytes 6291464 | tf_op jit(solution)/shard_map/ppermute | solution.py:18
  79.2 1.3 copy-start.3
  80.5 70.4 %collective-permute-start.2 = (bf16[4,2048,128]{2,1,0:T(8,128)(2,1)S(1)}, bf16[4,2048,128]{2,1,0:T(8,128)(2,1)S(1)}, u32[]{:S(2)}, u32[]{:S(2)}) collective-permute-start(bf16[4,2048,128]{2,1,0:T(8,128)(2,1)S(1)} %collective-permute-done.1), channel_id=1, source_target_pairs={{0,1},{1,2},{2,3},{3,4},{4,5},{5,6},{6,7},{7,0},{8,9},{9,10},{10,1... | collective-permute-start | bytes 6291464 | tf_op jit(solution)/shard_map/ppermute | solution.py:18
  150.9 1.4 copy-start.5
  152.3 67.8 %collective-permute-start.3 = (bf16[4,2048,128]{2,1,0:T(8,128)(2,1)S(1)}, bf16[4,2048,128]{2,1,0:T(8,128)(2,1)S(1)}, u32[]{:S(2)}, u32[]{:S(2)}) collective-permute-start(bf16[4,2048,128]{2,1,0:T(8,128)(2,1)S(1)} %collective-permute-done.2), channel_id=1, source_target_pairs={{0,1},{1,2},{2,3},{3,4},{4,5},{5,6},{6,7},{7,0},{8,9},{9,10},{10,1... | collective-permute-start | bytes 6291464 | tf_op jit(solution)/shard_map/ppermute | solution.py:18
  220.0 1.4 copy-start.7
  221.4 70.4 %collective-permute-start.4 = (bf16[4,2048,128]{2,1,0:T(8,128)(2,1)S(1)}, bf16[4,2048,128]{2,1,0:T(8,128)(2,1)S(1)}, u32[]{:S(2)}, u32[]{:S(2)}) collective-permute-start(bf16[4,2048,128]{2,1,0:T(8,128)(2,1)S(1)} %collective-permute-done.3), channel_id=1, source_target_pairs={{0,1},{1,2},{2,3},{3,4},{4,5},{5,6},{6,7},{7,0},{8,9},{9,10},{10,1... | collective-permute-start | bytes 6291464 | tf_op jit(solution)/shard_map/ppermute | solution.py:18
  291.8 1.3 copy-start.9
  293.1 71.5 %collective-permute-start.5 = (bf16[4,2048,128]{2,1,0:T(8,128)(2,1)S(1)}, bf16[4,2048,128]{2,1,0:T(8,128)(2,1)}, u32[]{:S(2)}, u32[]{:S(2)}) collective-permute-start(bf16[4,2048,128]{2,1,0:T(8,128)(2,1)S(1)} %collective-permute-done.4), channel_id=1, source_target_pairs={{0,1},{1,2},{2,3},{3,4},{4,5},{5,6},{6,7},{7,0},{8,9},{9,10},{10,1... | collective-permute-start | bytes 6291464 | tf_op jit(solution)/shard_map/ppermute | solution.py:18
  364.5 66.6 %collective-permute-start.6 = (bf16[4,2048,128]{2,1,0:T(8,128)(2,1)}, bf16[4,2048,128]{2,1,0:T(8,128)(2,1)}, u32[]{:S(2)}, u32[]{:S(2)}) collective-permute-start(bf16[4,2048,128]{2,1,0:T(8,128)(2,1)} %collective-permute-done.5), channel_id=1, source_target_pairs={{0,1},{1,2},{2,3},{3,4},{4,5},{5,6},{6,7},{7,0},{8,9},{9,10},{10,1... | collective-permute-start | bytes 6291464 | tf_op jit(solution)/shard_map/ppermute | solution.py:18
  376.5 3.9 copy-start.13
  376.5 56.0 %all-to-all-start.1 = ((bf16[16,48,2048]{2,1,0:T(8,128)(2,1)}), bf16[16,48,2048]{2,1,0:T(8,128)(2,1)S(1)}, u32[]{:S(2)}, u32[]{:S(2)}) async-start(bf16[16,48,2048]{2,1,0:T(8,128)(2,1)} %bitcast.7), calls=%async_computation.1 | async-start | bytes 6291456 | tf_op jit(solution)/shard_map/all_to_all | solution.py:102
  380.3 51.1 %copy-start.17 = (f32[128]{0:T(128)S(1)}, f32[128]{0:T(128)}, u32[]{:S(2)}) copy-start(f32[128]{0:T(128)} %param.11) | copy-start | bytes 1540
  380.3 169.3 %all-gather.4.cloned.1.call-start = ((), (), s32[]{:S(2)}) async-start(), calls=%async_computation.3 | async-start | bytes 4718592 | tf_op jit(solution)/shard_map/all_gather | solution.py:88
  380.4 50.8 %collective-permute-start = (bf16[15,128]{1,0:T(8,128)(2,1)S(1)}, bf16[15,128]{1,0:T(8,128)(2,1)S(1)}, u32[]{:S(2)}, u32[]{:S(2)}) collective-permute-start(bf16[15,128]{1,0:T(8,128)(2,1)S(1)} %slice.57), channel_id=1, source_target_pairs={{0,8},{8,16},{16,24},{1,9},{9,17},{17,25},{2,10},{10,18},{18,26},{... | collective-permute-start | bytes 11528 | tf_op jit(solution)/shard_map/ppermute | solution.py:31
  431.1 63.7 %collective-permute-start.7 = (bf16[4,2048,128]{2,1,0:T(8,128)(2,1)}, bf16[4,2048,128]{2,1,0:T(8,128)(2,1)}, u32[]{:S(2)}, u32[]{:S(2)}) collective-permute-start(bf16[4,2048,128]{2,1,0:T(8,128)(2,1)} %collective-permute-done.6), channel_id=1, source_target_pairs={{0,1},{1,2},{2,3},{3,4},{4,5},{5,6},{6,7},{7,0},{8,9},{9,10},{10,1... | collective-permute-start | bytes 6291464 | tf_op jit(solution)/shard_map/ppermute | solution.py:18
  432.5 4.5 copy-start
  432.5 111.5 %all-to-all-start = ((bf16[8,128,128]{2,1,0:T(8,128)(2,1)}), bf16[8,128,128]{2,1,0:T(8,128)(2,1)S(1)}, u32[]{:S(2)}, u32[]{:S(2)}) async-start(bf16[8,128,128]{2,1,0:T(8,128)(2,1)} %bitcast), calls=%async_computation | async-start | bytes 524288 | tf_op jit(solution)/shard_map/all_to_all | solution.py:85
  501.5 3.5 copy-start.10
  505.0 1.8 copy-start.8
  506.8 1.8 copy-start.6
  508.6 1.8 copy-start.4
  510.4 1.9 copy-start.2
  543.9 4.6 copy-start.16
  543.9 0.7 copy-start.12
  544.6 24.5 %all-to-all-start.2 = ((bf16[4,192,2048]{2,0,1:T(4,128)(2,1)}), bf16[4,192,2048]{2,0,1:T(4,128)(2,1)S(1)}, u32[]{:S(2)}, u32[]{:S(2)}) async-start(bf16[4,192,2048]{2,0,1:T(4,128)(2,1)} %copy.52), calls=%async_computation.2 | async-start | bytes 6291456 | tf_op jit(solution)/shard_map/all_to_all | solution.py:118
Sparse Core Ops, SparseCore 0:
  9.6 209.1 all-gather.5
  220.3 209.8 all-gather.7
  431.8 51.0 all-gather.3
